TPU v7x, 32 devices: a whole 2x2x4 slice. The times are simulated.
32 devices in a mesh: sp: 4 (over y, core), dp: 8 (over z, x).
Axes of the slice: x: 2, y: 2, z: 4, core: 2. Of those that a mesh axis runs over, the one named last changes fastest.
Arguments:
- q_latent: bfloat16 [8, 512, 512], P('dp', 'sp'), may hold values from -70 to 70
- kv_latent: bfloat16 [8, 512, 512], P('dp', 'sp'), may hold values from -70 to 70
- rope_key: bfloat16 [8, 512, 64], P('dp', 'sp'), may hold values from -370 to 370
- w_query: bfloat16 [512, 3072], P(None, 'dp'), may hold values from -0.25 to 0.25
- w_keyval: bfloat16 [512, 4096], P(None, 'sp'), may hold values from -0.25 to 0.25
- w_out: bfloat16 [2048, 2048], replicated, may hold values from -0.125 to 0.125
- query_gain: bfloat16 [512], replicated, may hold values from 0.099609375 to 1.8984375
- latent_gain: bfloat16 [512], replicated, may hold values from 0.099609375 to 1.8984375
- out_gain: bfloat16 [2048], replicated, may hold values from 0.099609375 to 1.8984375
Outputs:
- output: bfloat16 [8, 512, 2048], P('dp', 'sp')
All inputs are finite; a program needn't handle non-finite values.
Results may differ from a plain program's by a relative error of at most 0.03.
The roundings to bfloat16 on the way count: a program that leaves them out, or rounds other values in their place, can miss the bound.
Values may be sent and summed in bfloat16 or wider, within the bound.
A program may use at most 64 MiB of HBM per device.

v0:
```python
import jax
import jax.numpy as jnp
from jax import lax
from jax.sharding import PartitionSpec as P

H = 16
NOPE = 128
ROPE = 64
VDIM = 128


def normalize(row_values, gain_vector):
    widened = row_values.astype(jnp.float32)
    return (
        widened
        * lax.rsqrt(jnp.mean(widened * widened, axis=-1, keepdims=True) + 1e-05)
        * gain_vector.astype(jnp.float32)
    )


def angles_for(positions, rope_width):
    half_width = rope_width // 2
    inverse = 10000.0 ** (-jnp.arange(half_width, dtype=jnp.float32) / half_width)
    return positions.astype(jnp.float32)[:, None] * inverse[None, :]


def turn(vectors, angles):
    half_width = vectors.shape[-1] // 2
    cosine = jnp.cos(angles)
    sine_value = jnp.sin(angles)
    low_half = vectors[..., :half_width]
    high_half = vectors[..., half_width:]
    return jnp.concatenate(
        [low_half * cosine - high_half * sine_value, high_half * cosine + low_half * sine_value],
        axis=-1,
    )


def attend(query_head, keyval_head, rope_all):
    length = query_head.shape[0]
    local_heads = query_head.shape[1] // (NOPE + ROPE)
    query_three = query_head.reshape(length, local_heads, NOPE + ROPE)
    keyval_three = keyval_head.reshape(length, local_heads, NOPE + VDIM)
    block_rows = min(512, length)
    score_scale = (NOPE + ROPE) ** (-0.5)
    pieces = []
    for block_index in range(length // block_rows):
        block_start = block_index * block_rows
        block_stop = block_start + block_rows
        query_block = query_three[block_start:block_stop]
        scores = jnp.einsum(
            "qhd,khd->hqk",
            query_block[..., :NOPE],
            keyval_three[:block_stop, :, :NOPE],
            preferred_element_type=jnp.float32,
        )
        scores = scores + jnp.einsum(
            "qhr,kr->hqk",
            query_block[..., NOPE:],
            rope_all[:block_stop],
            preferred_element_type=jnp.float32,
        )
        scores = scores * score_scale
        allowed = jnp.arange(block_stop)[None, :] <= (block_start + jnp.arange(block_rows))[:, None]
        scores = jnp.where(allowed[None], scores, -jnp.inf)
        row_top = jnp.max(scores, axis=-1, keepdims=True)
        exponent = jnp.exp(scores - row_top)
        row_total = jnp.sum(exponent, axis=-1)
        summed = jnp.einsum(
            "hqk,khd->qhd",
            exponent.astype(jnp.bfloat16),
            keyval_three[:block_stop, :, NOPE:],
            preferred_element_type=jnp.float32,
        )
        pieces.append((summed / jnp.transpose(row_total)[:, :, None]).astype(jnp.bfloat16))
    return jnp.concatenate(pieces, axis=0).reshape(length, local_heads * VDIM)


def per_device(
    q_latent, kv_latent, rope_key, w_query, w_keyval, w_out, query_gain, latent_gain, out_gain
):
    tokens_here = q_latent.shape[1]
    offset = lax.axis_index("sp") * tokens_here
    positions = offset + jnp.arange(tokens_here, dtype=jnp.int32)
    angles = angles_for(positions, ROPE)
    query_norm = normalize(q_latent[0], query_gain).astype(jnp.bfloat16)
    query_raw = jnp.dot(
        query_norm,
        lax.all_gather(w_query, "dp", axis=1, tiled=True),
        preferred_element_type=jnp.float32,
    )
    query_raw = query_raw.reshape(tokens_here, H, NOPE + ROPE)
    queries = jnp.concatenate(
        [query_raw[..., :NOPE], turn(query_raw[..., NOPE:], angles[:, None, :])], axis=-1
    )
    queries = queries.astype(jnp.bfloat16).reshape(tokens_here, H * (NOPE + ROPE))
    latent_norm = normalize(kv_latent[0], latent_gain).astype(jnp.bfloat16)
    rope_turned = turn(rope_key[0].astype(jnp.float32), angles).astype(jnp.bfloat16)
    query_head = lax.all_to_all(queries, "sp", split_axis=1, concat_axis=0, tiled=True)
    latent_all, rope_all = (
        lax.all_gather(latent_norm, "sp", axis=0, tiled=True),
        lax.all_gather(rope_turned, "sp", axis=0, tiled=True),
    )
    keyval_head = jnp.dot(latent_all, w_keyval, preferred_element_type=jnp.float32).astype(
        jnp.bfloat16
    )
    attended = attend(query_head, keyval_head, rope_all)
    returned = lax.all_to_all(attended, "sp", split_axis=0, concat_axis=1, tiled=True)
    mixed_norm = normalize(returned, out_gain).astype(jnp.bfloat16)
    result = jnp.dot(mixed_norm, w_out, preferred_element_type=jnp.float32).astype(jnp.bfloat16)
    return result[None]


def solution(mesh):
    in_specs = (
        P("dp", "sp", None),
        P("dp", "sp", None),
        P("dp", "sp", None),
        P(None, "dp"),
        P(None, "sp"),
        P(),
        P(),
        P(),
        P(),
    )
    out_specs = P("dp", "sp", None)
    return jax.shard_map(
        per_device, mesh=mesh, in_specs=in_specs, out_specs=out_specs, check_vma=False
    )
```

profile of v0, /device:TPU:0, one launch (start us, length us, event | category | flops | bytes accessed | tf_op | source)
XLA Modules:
  0.0 132.7 jit_solution(3271215150385826949)
XLA Ops:
  6.5 0.7 all-gather.2.cloned.1.call-update
  7.3 0.7 convert_element_type.83
  7.9 0.7 convert_element_type.79
  8.6 1.0 fusion.23
  9.7 1.0 fusion.26
  10.7 1.0 fusion.28
  11.7 8.7 %all_gather.9 = bf16[512,512]{1,0:T(8,128)(2,1)S(1)} all-gather(bf16[128,512]{1,0:T(8,128)(2,1)S(1)} %fusion.28), channel_id=1, replica_groups=mesh['sp'=4,'dp'=8] {'sp'}, dimensions={0}, use_global_device_ids=true | all-gather | bytes 655360 | tf_op jit(solution)/shard_map/all_gather | solution.py:101
  20.4 0.7 bitcast_convert_fusion
  21.1 0.1 subtract_convert_fusion.1
  21.3 53.5 %all-gather.2.cloned.1.call-done = bf16[512,3072]{1,0:T(8,128)(2,1)} async-done(((bf16[512,384]{1,0:T(8,128)(2,1)}), bf16[512,3072]{1,0:T(8,128)(2,1)}) %all-gather.2.cloned.1.call-update) | async-done | bytes 3145744 | tf_op jit(solution)/shard_map/all_gather | solution.py:89
  74.8 4.7 %copy.23 = bf16[3072,512]{1,0:T(8,128)(2,1)} copy(bf16[3072,512]{0,1:T(8,128)(2,1)} %bitcast.53) | data formatting | bytes 6291456 | tf_op jit(solution)/shard_map/dot_general | solution.py:87
  79.5 2.9 %fusion.31 = f32[128,16,192]{0,2,1:T(8,128)S(1)} fusion(bf16[16,192,512]{2,1,0:T(8,128)(2,1)} %bitcast.52, bf16[1,128,512]{2,1,0:T(8,128)(2,1)S(1)} %copy-done.2, f32[512]{0:T(512)S(1)} %convert_element_type.83, f32[128]{0:T(128)S(1)} %add_rsqrt_fusion.1), kind=kOutput, calls=%fused_computation.39 | convolution fusion | flops 402915328 | bytes 4852224 | tf_op jit(solution)/shard_map/dot_general | solution.py:87
  82.6 1.0 pad_maximum_fusion
  83.6 3.5 %all-to-all-start = ((bf16[128,4,768]{0,2,1:T(8,128)(2,1)}), bf16[128,4,768]{0,2,1:T(8,128)(2,1)S(1)}, u32[]{:S(2)}, u32[]{:S(2)}) async-start(bf16[128,4,768]{0,2,1:T(8,128)(2,1)} %bitcast.6), calls=%async_computation | async-start | bytes 1572864 | tf_op jit(solution)/shard_map/all_to_all | solution.py:99
  87.1 1.7 %convolution_convert_fusion.1 = bf16[512,1024]{1,0:T(8,128)(2,1)} fusion(bf16[512,512]{1,0:T(8,128)(2,1)S(1)} %all_gather.9, bf16[512,1024]{1,0:T(8,128)(2,1)S(1)} %copy-done), kind=kOutput, calls=%fused_computation.10 | convolution fusion | flops 537395200 | bytes 2621440 | tf_op jit(solution)/shard_map/dot_general | solution.py:104
  88.8 1.9 %reshape.144 = bf16[512,4,256]{2,1,0:T(4,128)(2,1)S(1)} reshape(bf16[512,1024]{1,0:T(8,128)(2,1)} %convolution_convert_fusion.1) | data formatting | bytes 2097152 | tf_op jit(solution)/shard_map/reshape | solution.py:43
  90.7 9.2 %all_gather.11 = bf16[512,64]{0,1:T(8,128)(2,1)S(1)} all-gather(bf16[128,64]{0,1:T(8,128)(2,1)S(1)} %pad_maximum_fusion.1), channel_id=1, replica_groups=mesh['sp'=4,'dp'=8] {'sp'}, dimensions={0}, use_global_device_ids=true | all-gather | bytes 81920 | tf_op jit(solution)/shard_map/all_gather | solution.py:102
  99.9 0.8 iota_compare_fusion
  100.7 1.2 fusion.36
  101.8 0.6 copy.24
  102.4 0.3 reshape.145
  102.7 0.7 fusion.19
  103.4 1.2 fusion.37
  104.6 0.6 fusion.2
  105.2 0.5 copy-done.3
  105.7 0.8 fusion.14
  106.6 0.9 copy.28
  107.4 3.5 %all-to-all-start.1 = ((bf16[4,128,512]{1,2,0:T(8,128)(2,1)}), bf16[4,128,512]{1,2,0:T(8,128)(2,1)S(1)}, u32[]{:S(2)}, u32[]{:S(2)}) async-start(bf16[4,128,512]{1,2,0:T(8,128)(2,1)} %copy.28), calls=%async_computation.1 | async-start | bytes 1048576 | tf_op jit(solution)/shard_map/all_to_all | solution.py:108
  111.0 8.8 %all-to-all-done.1 = bf16[4,128,512]{1,2,0:T(8,128)(2,1)S(1)} async-done(((bf16[4,128,512]{1,2,0:T(8,128)(2,1)}), bf16[4,128,512]{1,2,0:T(8,128)(2,1)S(1)}, u32[]{:S(2)}, u32[]{:S(2)}) %all-to-all-start.1) | async-done | bytes 524320 | tf_op jit(solution)/shard_map/all_to_all | solution.py:108
  119.7 0.3 multiply_reduce_fusion
  120.0 0.3 fusion.18
  120.4 5.5 %fusion.4 = bf16[1,128,2048]{2,1,0:T(8,128)(2,1)} fusion(bf16[128,2048]{0,1:T(8,128)(2,1)S(1)} %fusion.18, bf16[2048,2048]{1,0:T(8,128)(2,1)} %param.14), kind=kOutput, calls=%fused_computation.7 | convolution fusion | flops 1074003968 | bytes 9437184 | tf_op jit(solution)/shard_map/dot_general | solution.py:110
  (21 shorter events, 0.3 us)
Async XLA Ops:
  6.5 80.6 %copy-start = (bf16[512,1024]{1,0:T(8,128)(2,1)S(1)}, bf16[512,1024]{1,0:T(8,128)(2,1)}, u32[]{:S(2)}) copy-start(bf16[512,1024]{1,0:T(8,128)(2,1)} %param.13) | copy-start | bytes 3145732
  6.5 73.0 %copy-start.2 = (bf16[1,128,512]{2,1,0:T(8,128)(2,1)S(1)}, bf16[1,128,512]{2,1,0:T(8,128)(2,1)}, u32[]{:S(2)}) copy-start(bf16[1,128,512]{2,1,0:T(8,128)(2,1)} %param.9) | copy-start | bytes 393220
  6.5 68.3 %all-gather.2.cloned.1.call-start = ((), (), s32[]{:S(2)}) async-start(), calls=%async_computation.2 | async-start | bytes 3538944 | tf_op jit(solution)/shard_map/all_gather | solution.py:89
  83.6 18.2 %all-to-all-start = ((bf16[128,4,768]{0,2,1:T(8,128)(2,1)}), bf16[128,4,768]{0,2,1:T(8,128)(2,1)S(1)}, u32[]{:S(2)}, u32[]{:S(2)}) async-start(bf16[128,4,768]{0,2,1:T(8,128)(2,1)} %bitcast.6), calls=%async_computation | async-start | bytes 1572864 | tf_op jit(solution)/shard_map/all_to_all | solution.py:99
  101.8 1.6 %copy-start.1 = (pred[512,512]{0,1:T(8,128)(4,1)S(1)}, pred[512,512]{0,1:T(8,128)(4,1)}, u32[]{:S(2)}) copy-start(pred[512,512]{0,1:T(8,128)(4,1)} %iota_compare_fusion) | copy-start | bytes 786436
  104.6 1.0 copy-start.3
  105.7 5.3 %copy-start.4 = (bf16[2048]{0:T(1024)(128)(2,1)S(1)}, bf16[2048]{0:T(1024)(128)(2,1)}, u32[]{:S(2)}) copy-start(bf16[2048]{0:T(1024)(128)(2,1)} %param.17) | copy-start | bytes 12292
  107.4 12.3 %all-to-all-start.1 = ((bf16[4,128,512]{1,2,0:T(8,128)(2,1)}), bf16[4,128,512]{1,2,0:T(8,128)(2,1)S(1)}, u32[]{:S(2)}, u32[]{:S(2)}) async-start(bf16[4,128,512]{1,2,0:T(8,128)(2,1)} %copy.28), calls=%async_computation.1 | async-start | bytes 1048576 | tf_op jit(solution)/shard_map/all_to_all | solution.py:108
Sparse Core Ops, SparseCore 0:
  9.4 65.3 all-gather.1
where the time goes:
time: 133 us
  waiting for transfers between devices  63 us (47%)
  blocking collectives  17.9 us (13%)
  between operations  13.6 us (10%)
  matrix products  12.7 us (10%)
  local copies, waits for them, and re-layouts  10.1 us (8%)
  other arithmetic  8.35 us (6%)
  starting transfers between devices  6.97 us (5%)
    all_gather x1, waiting for transfers between devices, per_device(): lax.all_gather(w_query, 'dp', axis=1, tiled=True)  53.5 us
    all_gather x1, blocking collectives, per_device(): lax.all_gather(rope_turned, 'sp', axis=0, tiled=True)  9.22 us
    all_to_all x1, waiting for transfers between devices, per_device(): lax.all_to_all(attended, 'sp', split_axis=0, concat_axis=1, tiled=True)  8.76 us
    all_gather x1, blocking collectives, per_device(): lax.all_gather(latent_norm, 'sp', axis=0, tiled=True)  8.68 us
    dot_general x1, matrix products, per_device(): jnp.dot(mixed_norm, w_out, preferred_element_type=jnp.float32)  5.47 us
    dot_general x1, local copies, waits for them, and re-layouts, per_device(): jnp.dot(query_norm, lax.all_gather(w_query, 'dp', axis=1, tiled=True), pr...  4.68 us
    all_to_all x1, starting transfers between devices, per_device(): lax.all_to_all(queries, 'sp', split_axis=1, concat_axis=0, tiled=True)  3.49 us
    all_to_all x1, starting transfers between devices, per_device(): lax.all_to_all(attended, 'sp', split_axis=0, concat_axis=1, tiled=True)  3.47 us
  transfers between devices with their start and end apart: 3, of which 2 were waited for; matrix products, arithmetic and copies ran while one was open for 8% of the time, Pallas kernels for 0%

commit v1 on v0

--- a/solution.py
+++ b/solution.py
@@ -105,7 +105,10 @@
         jnp.bfloat16
     )
     attended = attend(query_head, keyval_head, rope_all)
-    returned = lax.all_to_all(attended, "sp", split_axis=0, concat_axis=1, tiled=True)
+    returned = jnp.concatenate(
+        lax.all_to_all(jnp.stack(jnp.split(attended, lax.axis_size("sp"), axis=0)), "sp", 0, 0),
+        axis=1,
+    )
     mixed_norm = normalize(returned, out_gain).astype(jnp.bfloat16)
     result = jnp.dot(mixed_norm, w_out, preferred_element_type=jnp.float32).astype(jnp.bfloat16)
     return result[None]

time: 133 us -> 133 us (level)
  no operation moved by 1% of the time
where the time goes in v1:
time: 133 us
  waiting for transfers between devices  63 us (47%)
  blocking collectives  17.9 us (13%)
  between operations  13.6 us (10%)
  matrix products  12.7 us (10%)
  local copies, waits for them, and re-layouts  9.27 us (7%)
  other arithmetic  9.21 us (7%)
  starting transfers between devices  6.97 us (5%)
    all_gather x1, waiting for transfers between devices, per_device(): lax.all_gather(w_query, 'dp', axis=1, tiled=True)  53.5 us
    all_gather x1, blocking collectives, per_device(): lax.all_gather(rope_turned, 'sp', axis=0, tiled=True)  9.23 us
    all_to_all x1, waiting for transfers between devices, per_device(): lax.all_to_all(jnp.stack(jnp.split(attended, lax.axis_size('sp'), axis=0)...  8.76 us
    all_gather x1, blocking collectives, per_device(): lax.all_gather(latent_norm, 'sp', axis=0, tiled=True)  8.68 us
    dot_general x1, matrix products, per_device(): jnp.dot(mixed_norm, w_out, preferred_element_type=jnp.float32)  5.47 us
    dot_general x1, local copies, waits for them, and re-layouts, per_device(): jnp.dot(query_norm, lax.all_gather(w_query, 'dp', axis=1, tiled=True), pr...  4.68 us
    all_to_all x1, starting transfers between devices, per_device(): lax.all_to_all(queries, 'sp', split_axis=1, concat_axis=0, tiled=True)  3.49 us
    all_to_all x1, starting transfers between devices, per_device(): lax.all_to_all(jnp.stack(jnp.split(attended, lax.axis_size('sp'), axis=0)...  3.47 us
  transfers between devices with their start and end apart: 3, of which 2 were waited for; matrix products, arithmetic and copies ran while one was open for 8% of the time, Pallas kernels for 0%

profile of v1, /device:TPU:0, one launch (start us, length us, event | category | flops | bytes accessed | tf_op | source)
XLA Modules:
  0.0 132.7 jit_solution(4825476354346039712)
XLA Ops:
  6.5 0.7 all-gather.2.cloned.1.call-update
  7.3 0.7 convert_element_type.83
  7.9 0.7 convert_element_type.79
  8.6 1.0 fusion.23
  9.7 1.0 fusion.26
  10.7 1.0 fusion.28
  11.7 8.7 %all_gather.9 = bf16[512,512]{1,0:T(8,128)(2,1)S(1)} all-gather(bf16[128,512]{1,0:T(8,128)(2,1)S(1)} %fusion.28), channel_id=1, replica_groups=mesh['sp'=4,'dp'=8] {'sp'}, dimensions={0}, use_global_device_ids=true | all-gather | bytes 655360 | tf_op jit(solution)/shard_map/all_gather | solution.py:101
  20.4 0.7 bitcast_convert_fusion
  21.1 0.1 subtract_convert_fusion.1
  21.3 53.5 %all-gather.2.cloned.1.call-done = bf16[512,3072]{1,0:T(8,128)(2,1)} async-done(((bf16[512,384]{1,0:T(8,128)(2,1)}), bf16[512,3072]{1,0:T(8,128)(2,1)}) %all-gather.2.cloned.1.call-update) | async-done | bytes 3145744 | tf_op jit(solution)/shard_map/all_gather | solution.py:89
  74.8 4.7 %copy.22 = bf16[3072,512]{1,0:T(8,128)(2,1)} copy(bf16[3072,512]{0,1:T(8,128)(2,1)} %bitcast.55) | data formatting | bytes 6291456 | tf_op jit(solution)/shard_map/dot_general | solution.py:87
  79.5 2.9 %fusion.31 = f32[128,16,192]{0,2,1:T(8,128)S(1)} fusion(bf16[16,192,512]{2,1,0:T(8,128)(2,1)} %bitcast.54, bf16[1,128,512]{2,1,0:T(8,128)(2,1)S(1)} %copy-done.2, f32[512]{0:T(512)S(1)} %convert_element_type.83, f32[128]{0:T(128)S(1)} %add_rsqrt_fusion.1), kind=kOutput, calls=%fused_computation.40 | convolution fusion | flops 402915328 | bytes 4852224 | tf_op jit(solution)/shard_map/dot_general | solution.py:87
  82.6 1.0 pad_maximum_fusion
  83.6 3.5 %all-to-all-start = ((bf16[128,4,768]{0,2,1:T(8,128)(2,1)}), bf16[128,4,768]{0,2,1:T(8,128)(2,1)S(1)}, u32[]{:S(2)}, u32[]{:S(2)}) async-start(bf16[128,4,768]{0,2,1:T(8,128)(2,1)} %bitcast.6), calls=%async_computation | async-start | bytes 1572864 | tf_op jit(solution)/shard_map/all_to_all | solution.py:99
  87.1 1.7 %convolution_convert_fusion.1 = bf16[512,1024]{1,0:T(8,128)(2,1)} fusion(bf16[512,512]{1,0:T(8,128)(2,1)S(1)} %all_gather.9, bf16[512,1024]{1,0:T(8,128)(2,1)S(1)} %copy-done), kind=kOutput, calls=%fused_computation.10 | convolution fusion | flops 537395200 | bytes 2621440 | tf_op jit(solution)/shard_map/dot_general | solution.py:104
  88.8 1.9 %reshape.150 = bf16[512,4,256]{2,1,0:T(4,128)(2,1)S(1)} reshape(bf16[512,1024]{1,0:T(8,128)(2,1)} %convolution_convert_fusion.1) | data formatting | bytes 2097152 | tf_op jit(solution)/shard_map/reshape | solution.py:43
  90.7 9.2 %all_gather.11 = bf16[512,64]{0,1:T(8,128)(2,1)S(1)} all-gather(bf16[128,64]{0,1:T(8,128)(2,1)S(1)} %pad_maximum_fusion.2), channel_id=1, replica_groups=mesh['sp'=4,'dp'=8] {'sp'}, dimensions={0}, use_global_device_ids=true | all-gather | bytes 81920 | tf_op jit(solution)/shard_map/all_gather | solution.py:102
  99.9 0.8 iota_compare_fusion
  100.7 1.2 fusion.36
  101.8 0.6 copy.23
  102.4 0.3 reshape.151
  102.7 0.7 fusion.19
  103.4 1.2 fusion.38
  104.6 0.6 fusion.2
  105.2 0.5 copy-done.3
  105.7 0.8 fusion.14
  106.6 0.9 pad_maximum_fusion.1
  107.4 3.5 %all-to-all-start.1 = ((bf16[4,128,512]{1,2,0:T(8,128)(2,1)}), bf16[4,128,512]{1,2,0:T(8,128)(2,1)S(1)}, u32[]{:S(2)}, u32[]{:S(2)}) async-start(bf16[4,128,512]{1,2,0:T(8,128)(2,1)} %pad_maximum_fusion.1), calls=%async_computation.1 | async-start | bytes 1048576 | tf_op jit(solution)/shard_map/all_to_all | solution.py:109
  110.9 8.8 %all-to-all-done.1 = bf16[4,128,512]{1,2,0:T(8,128)(2,1)S(1)} async-done(((bf16[4,128,512]{1,2,0:T(8,128)(2,1)}), bf16[4,128,512]{1,2,0:T(8,128)(2,1)S(1)}, u32[]{:S(2)}, u32[]{:S(2)}) %all-to-all-start.1) | async-done | bytes 524320 | tf_op jit(solution)/shard_map/all_to_all | solution.py:109
  119.7 0.3 multiply_reduce_fusion
  120.0 0.3 fusion.18
  120.3 5.5 %fusion.4 = bf16[1,128,2048]{2,1,0:T(8,128)(2,1)} fusion(bf16[128,2048]{0,1:T(8,128)(2,1)S(1)} %fusion.18, bf16[2048,2048]{1,0:T(8,128)(2,1)} %param.14), kind=kOutput, calls=%fused_computation.7 | convolution fusion | flops 1074003968 | bytes 9437184 | tf_op jit(solution)/shard_map/dot_general | solution.py:113
  (21 shorter events, 0.3 us)
Async XLA Ops:
  6.5 80.6 %copy-start = (bf16[512,1024]{1,0:T(8,128)(2,1)S(1)}, bf16[512,1024]{1,0:T(8,128)(2,1)}, u32[]{:S(2)}) copy-start(bf16[512,1024]{1,0:T(8,128)(2,1)} %param.13) | copy-start | bytes 3145732
  6.5 73.0 %copy-start.2 = (bf16[1,128,512]{2,1,0:T(8,128)(2,1)S(1)}, bf16[1,128,512]{2,1,0:T(8,128)(2,1)}, u32[]{:S(2)}) copy-start(bf16[1,128,512]{2,1,0:T(8,128)(2,1)} %param.9) | copy-start | bytes 393220
  6.5 68.3 %all-gather.2.cloned.1.call-start = ((), (), s32[]{:S(2)}) async-start(), calls=%async_computation.2 | async-start | bytes 3538944 | tf_op jit(solution)/shard_map/all_gather | solution.py:89
  83.6 18.2 %all-to-all-start = ((bf16[128,4,768]{0,2,1:T(8,128)(2,1)}), bf16[128,4,768]{0,2,1:T(8,128)(2,1)S(1)}, u32[]{:S(2)}, u32[]{:S(2)}) async-start(bf16[128,4,768]{0,2,1:T(8,128)(2,1)} %bitcast.6), calls=%async_computation | async-start | bytes 1572864 | tf_op jit(solution)/shard_map/all_to_all | solution.py:99
  101.8 1.6 %copy-start.1 = (pred[512,512]{0,1:T(8,128)(4,1)S(1)}, pred[512,512]{0,1:T(8,128)(4,1)}, u32[]{:S(2)}) copy-start(pred[512,512]{0,1:T(8,128)(4,1)} %iota_compare_fusion) | copy-start | bytes 786436
  104.6 1.0 copy-start.3
  105.7 5.3 %copy-start.4 = (bf16[2048]{0:T(1024)(128)(2,1)S(1)}, bf16[2048]{0:T(1024)(128)(2,1)}, u32[]{:S(2)}) copy-start(bf16[2048]{0:T(1024)(128)(2,1)} %param.17) | copy-start | bytes 12292
  107.4 12.3 %all-to-all-start.1 = ((bf16[4,128,512]{1,2,0:T(8,128)(2,1)}), bf16[4,128,512]{1,2,0:T(8,128)(2,1)S(1)}, u32[]{:S(2)}, u32[]{:S(2)}) async-start(bf16[4,128,512]{1,2,0:T(8,128)(2,1)} %pad_maximum_fusion.1), calls=%async_computation.1 | async-start | bytes 1048576 | tf_op jit(solution)/shard_map/all_to_all | solution.py:109
Sparse Core Ops, SparseCore 0:
  9.4 65.3 all-gather.1
